TPU v7x, 128 devices: a whole 4x4x4 slice. The times are simulated.
128 devices in a mesh: sp: 16 (over z, y), tp: 8 (over x, core).
Axes of the slice: x: 4, y: 4, z: 4, core: 2. Of those that a mesh axis runs over, the one named last changes fastest.
Arguments:
- target: bfloat16 [4096, 2048], P(('sp', 'tp')), may hold values from -6 to 6
- source: bfloat16 [8192, 2048], P(('sp', 'tp')), may hold values from -6 to 6
- target_gain: bfloat16 [2, 2048], replicated, may hold values from 0.099609375 to 1.8984375
- source_gain: bfloat16 [2, 2048], replicated, may hold values from 0.099609375 to 1.8984375
- query_w: bfloat16 [2, 2048, 8192], P(None, None, 'tp'), may hold values from -0.125 to 0.125
- key_w: bfloat16 [2, 2048, 4096], P(None, None, 'tp'), may hold values from -0.125 to 0.125
- value_w: bfloat16 [2, 2048, 4096], P(None, None, 'tp'), may hold values from -0.125 to 0.125
- out_w: bfloat16 [2, 8192, 2048], P(None, 'tp'), may hold values from -0.1875 to 0.1875
- head_temp: float32 [2, 16], P(None, 'tp'), may hold values from 1.5 to 8, as said below
- final_gain: bfloat16 [2048], replicated, may hold values from 0.099609375 to 1.8984375
Outputs:
- result: float32 [4096, 2048], P(('sp', 'tp'))
Inputs may be any that keep to these rules, and one draw needn't show every extreme that they name: `head_temp`: a positive scale for each head's scores.
All inputs are finite; a program needn't handle non-finite values.
Results may differ from a plain program's by a relative error of at most 0.04.
Values may be sent and summed in bfloat16 or wider, within the bound.
A program may use at most 192 MiB of HBM per device.

v0:
```python
import jax
import jax.numpy as jnp
from jax import lax
from jax.sharding import Mesh
from jax.sharding import PartitionSpec as P

HEAD_DIM = 512
TP = ("tp_0", "tp_1")
SP_TP = ("sp", "tp_0", "tp_1")
EPS = 1e-06
FLOOR = -1e30


def laid_out(pieces, dim):
    shape = list(pieces.shape[1:])
    shape[dim] *= pieces.shape[0]
    return jnp.moveaxis(pieces, 0, dim).reshape(shape)


def copy_for_each(shard, axis):
    copies = jnp.broadcast_to(shard, (lax.axis_size(axis), *shard.shape))
    return lax.all_to_all(copies, axis, split_axis=0, concat_axis=0, tiled=True)


def collect(shard, axis, dim):
    return laid_out(copy_for_each(shard, axis), dim)


def cut_rows(length, count):
    hop = length // count
    if hop >= 8:
        hop -= hop % 8
    return [hop * k for k in range(1, count)]


def gather_in_order(shard, axes, order):
    pieces = shard
    for k in order:
        pieces = lax.all_gather(pieces, axes[k])
    done = order[::-1]
    back = [done.index(k) for k in range(len(axes))]
    pieces = pieces.transpose(*back, *range(len(axes), pieces.ndim))
    return pieces.reshape(-1, *shard.shape)


def gather_at_once(shard, axes, dim):
    numbers = list(range(len(axes)))[::-1]
    widest = shard.shape.index(max(shard.shape[:-1] or shard.shape))
    edges = [0, *cut_rows(shard.shape[widest], len(axes)), shard.shape[widest]]
    gathered = []
    for k, (start, end) in enumerate(zip(edges, edges[1:])):
        if end > start:
            share = lax.slice_in_dim(shard, start, end, axis=widest)
            gathered.append(gather_in_order(share, axes, numbers[k:] + numbers[:k]))
    return laid_out(jnp.concatenate(gathered, axis=widest + 1), dim)


def cut_along(shard, dim, count):
    shape = shard.shape
    pieces = shard.reshape(*shape[:dim], count, shape[dim] // count, *shape[dim + 1 :])
    return jnp.moveaxis(pieces, dim, 0)


def summed_on_arrival(shard, axis, dim):
    count = lax.axis_size(axis)
    pieces = lax.all_to_all(cut_along(shard, dim, count), axis, 0, 0, tiled=True)
    return jnp.sum(pieces.astype(jnp.float32), axis=0)


def unit_rows(matrix):
    values = matrix.astype(jnp.float32)
    return values * lax.rsqrt(jnp.mean(values * values, axis=-1, keepdims=True) + EPS)


def per_device(
    target, source, target_gain, source_gain, query_w, key_w, value_w, out_w, head_temp, final_gain
):
    local_heads = query_w.shape[2] // HEAD_DIM
    local_shared = key_w.shape[2] // HEAD_DIM
    group_size = local_heads // local_shared
    shared_width = key_w.shape[2]
    source_gains = source_gain.astype(jnp.float32)
    unit_piece = unit_rows(collect(source, TP, 0))
    outputs = []
    for project_layer_index in range(2):
        project_normed = (unit_piece * source_gains[project_layer_index]).astype(jnp.bfloat16)
        outputs.append(
            jnp.dot(
                project_normed, key_w[project_layer_index], preferred_element_type=jnp.float32
            ).astype(jnp.bfloat16)
        )
        outputs.append(
            jnp.dot(
                project_normed, value_w[project_layer_index], preferred_element_type=jnp.float32
            ).astype(jnp.bfloat16)
        )
    projected = jnp.concatenate(outputs, axis=1)
    hidden_state = target.astype(jnp.float32)
    for layer_index in range(2):
        key_rows = projected[
            :, 2 * layer_index * shared_width : (2 * layer_index + 1) * shared_width
        ]
        value_rows = projected[
            :, (2 * layer_index + 1) * shared_width : (2 * layer_index + 2) * shared_width
        ]
        normed = (unit_rows(hidden_state) * target_gain[layer_index].astype(jnp.float32)).astype(
            jnp.bfloat16
        )
        queries = jnp.dot(
            gather_at_once(normed, TP, 0), query_w[layer_index], preferred_element_type=jnp.float32
        ).astype(jnp.bfloat16)
        row_count = queries.shape[0]
        query_view = queries.reshape(row_count, local_shared, group_size, HEAD_DIM)
        scales = (head_temp[layer_index] * HEAD_DIM ** (-0.5)).reshape(local_shared, group_size)
        start_max = jnp.full((row_count, local_shared, group_size), FLOOR, jnp.float32)
        row_max = start_max
        key_view = lax.all_gather(key_rows, "sp", axis=0, tiled=True).reshape(
            -1, local_shared, HEAD_DIM
        )
        value_view = lax.all_gather(value_rows, "sp", axis=0, tiled=True).reshape(
            -1, local_shared, HEAD_DIM
        )
        scores = jnp.einsum(
            "tkgd,nkd->tkgn", query_view, key_view, preferred_element_type=jnp.float32
        )
        scores = scores * scales[None, :, :, None]
        new_max = jnp.maximum(row_max, jnp.max(scores, axis=-1))
        exponent = jnp.exp(scores - new_max[..., None])
        row_total = jnp.sum(exponent, axis=-1)
        accumulated = jnp.einsum(
            "tkgn,nkd->tkgd",
            exponent.astype(jnp.bfloat16),
            value_view,
            preferred_element_type=jnp.float32,
        )
        row_max, row_total, accumulated = (new_max, row_total, accumulated)
        attended = (accumulated / row_total[..., None]).astype(jnp.bfloat16)
        flat_heads = attended.reshape(row_count, local_heads * HEAD_DIM)
        mixed = summed_on_arrival(
            jnp.dot(flat_heads, out_w[layer_index], preferred_element_type=jnp.float32).astype(
                jnp.bfloat16
            ),
            TP,
            0,
        )
        hidden_state = hidden_state + mixed
    return unit_rows(hidden_state) * final_gain.astype(jnp.float32)


def solution(mesh):
    split = Mesh(mesh.devices.reshape(mesh.shape["sp"], 4, 2), ("sp", "tp_0", "tp_1"))
    in_specs = (
        P(SP_TP, None),
        P(SP_TP, None),
        P(),
        P(),
        P(None, None, TP),
        P(None, None, TP),
        P(None, None, TP),
        P(None, TP, None),
        P(None, TP),
        P(),
    )
    out_specs = P(SP_TP, None)
    return jax.shard_map(
        per_device, mesh=split, in_specs=in_specs, out_specs=out_specs, check_vma=False
    )
```

profile of v0, /device:TPU:1, one launch (start us, length us, event | category | flops | bytes accessed | tf_op | source)
XLA Modules:
  0.0 381.8 jit_solution(2791178233135704088)
XLA Ops:
  6.5 2.6 broadcast_in_dim.2
  9.1 5.8 %all-to-all-start = ((bf16[8,64,2048]{2,1,0:T(8,128)(2,1)}), bf16[8,64,2048]{2,1,0:T(8,128)(2,1)S(1)}, u32[]{:S(2)}, u32[]{:S(2)}) async-start(bf16[8,64,2048]{2,1,0:T(8,128)(2,1)} %broadcast_in_dim.2), calls=%async_computation | async-start | bytes 4194304 | tf_op jit(solution)/shard_map/all_to_all | solution.py:22
  14.9 26.2 %all-to-all-done = bf16[8,64,2048]{2,1,0:T(8,128)(2,1)S(1)} async-done(((bf16[8,64,2048]{2,1,0:T(8,128)(2,1)}), bf16[8,64,2048]{2,1,0:T(8,128)(2,1)S(1)}, u32[]{:S(2)}, u32[]{:S(2)}) %all-to-all-start) | async-done | bytes 2097184 | tf_op jit(solution)/shard_map/all_to_all | solution.py:22
  41.1 0.5 fusion.26
  41.6 2.1 fusion.24
  43.7 1.3 copy-done.2
  45.0 2.1 fusion.70
  47.1 0.0 all-gather.13.cloned.1.call-start
  47.2 4.4 %fusion.67 = bf16[512,512]{1,0:T(8,128)(2,1)} fusion(bf16[512,2048]{1,0:T(8,128)(2,1)} %bitcast.231, bf16[2,2048,512]{2,1,0:T(8,128)(2,1)} %param.16), kind=kOutput, calls=%fused_computation.63 | convolution fusion | flops 1074003968 | bytes 4718592 | tf_op jit(solution)/shard_map/dot_general | solution.py:93
  51.6 0.0 all-gather.19.cloned.1.call-start
  51.7 3.7 fusion.76
  55.4 0.0 all-gather.17.cloned.1.call-start
  55.4 3.7 fusion.73
  59.1 0.1 fusion.109
  59.3 0.1 fusion.111
  59.4 10.6 %all-gather.2 = bf16[64,2048]{1,0:T(8,128)(2,1)S(1)} all-gather(bf16[16,2048]{1,0:T(8,128)(2,1)S(1)} %get-tuple-element.10), channel_id=4, replica_groups=mesh['sp'=16,'tp_0'=4,'tp_1'=2] {'tp_0'}, dimensions={0}, use_global_device_ids=true | all-gather | bytes 327680 | tf_op jit(solution)/shard_map/all_gather | solution.py:39
  70.0 4.6 %all-gather.3 = bf16[8,16,2048]{2,1,0:T(8,128)(2,1)S(1)} all-gather(bf16[4,16,2048]{2,1,0:T(8,128)(2,1)S(1)} %bitcast.232), channel_id=5, replica_groups=mesh['sp'=16,'tp_0'=4,'tp_1'=2] {'tp_1'}, dimensions={0}, use_global_device_ids=true | all-gather | bytes 786432 | tf_op jit(solution)/shard_map/all_gather | solution.py:39
  74.6 1.9 all-gather
  76.5 10.5 %all-gather.1 = bf16[8,16,2048]{2,1,0:T(8,128)(2,1)S(1)} all-gather(bf16[2,16,2048]{2,1,0:T(8,128)(2,1)S(1)} %bitcast.237), channel_id=3, replica_groups=mesh['sp'=16,'tp_0'=4,'tp_1'=2] {'tp_0'}, dimensions={0}, use_global_device_ids=true | all-gather | bytes 655360 | tf_op jit(solution)/shard_map/all_gather | solution.py:39
  87.0 0.1 pad_maximum_fusion
  87.1 3.5 fusion.79
  90.6 28.3 %all-gather.15.cloned.1.call-done = bf16[8192,512]{1,0:T(8,128)(2,1)} async-done(((bf16[512,512]{1,0:T(8,128)(2,1)}), bf16[8192,512]{1,0:T(8,128)(2,1)}) %all-gather.15.cloned.1.call-update) | async-done | bytes 8388624 | tf_op jit(solution)/shard_map/all_gather | solution.py:117
  118.9 11.6 %bitcast_reduce_fusion.1 = (f32[256,2]{0,1:T(2,128)S(1)}, f32[8192,256,2]{1,0,2:T(8,128)}) fusion(f32[2]{0:T(128)S(1)} %get-tuple-element.16, bf16[32,2,8,512]{3,2,1,0:T(8,128)(2,1)S(1)} %bitcast.246, bf16[8192,512]{1,0:T(8,128)(2,1)} %all-gather.15.cloned.1.call-done), kind=kOutput, calls=%fused_computation.5 | convolution fusion | flops 4303355392 | bytes 25692168 | tf_op jit(solution)/shard_map/tkgd,nkd->tkgn/dot_general | solution.py:123
  130.5 8.9 %fusion.2 = f32[256,2]{0,1:T(2,128)S(1)} fusion(f32[8192,256,2]{1,0,2:T(8,128)} %get-tuple-element.18, f32[256,2]{0,1:T(2,128)S(1)} %broadcast_maximum_fusion.1, f32[2]{0:T(128)S(1)} %get-tuple-element.16), kind=kLoop, calls=%fused_computation.8 | loop fusion | flops 12582400 | bytes 16781320 | tf_op jit(solution)/shard_map/reduce_sum | solution.py:129
  139.4 52.2 %all-gather.13.cloned.1.call-done = bf16[8192,512]{1,0:T(8,128)(2,1)} async-done(((bf16[512,512]{1,0:T(8,128)(2,1)}), bf16[8192,512]{1,0:T(8,128)(2,1)}) %all-gather.13.cloned.1.call-update) | async-done | bytes 8388624 | tf_op jit(solution)/shard_map/all_gather | solution.py:120
  191.6 12.8 %fusion.100 = bf16[1,512,256,2]{2,1,3,0:T(8,128)(2,1)S(1)} fusion(f32[8192,256,2]{1,0,2:T(8,128)} %get-tuple-element.18, f32[256,2]{0,1:T(2,128)S(1)} %broadcast_maximum_fusion.1, f32[2]{0:T(128)S(1)} %get-tuple-element.16, bf16[8192,512]{1,0:T(8,128)(2,1)} %all-gather.13.cloned.1.call-done, f32[256,2]{0,1:T(2,128)S(1)} %fusion.2), kind=kOutput, calls=%fused_computation.72 | convolution fusion | flops 4308074496 | bytes 25694216 | tf_op jit(solution)/shard_map/tkgn,nkd->tkgd/dot_general | solution.py:130
  204.4 3.7 fusion.39
  208.1 20.0 %all_to_all.15 = bf16[8,32,2048]{2,1,0:T(8,128)(2,1)S(1)} all-to-all(bf16[8,32,2048]{2,1,0:T(8,128)(2,1)S(1)} %bitcast.236), channel_id=1, replica_groups=mesh['sp'=16,'tp_0'=4,'tp_1'=2] {'tp_0','tp_1'}, dimensions={0} | all-to-all | bytes 2097152 | tf_op jit(solution)/shard_map/all_to_all | solution.py:66
  228.1 0.1 convert_reduce_fusion.1
  228.3 0.1 multiply_reduce_fusion.1
  228.4 0.1 multiply_convert_fusion
  228.6 10.6 %all-gather.6 = bf16[64,2048]{1,0:T(8,128)(2,1)S(1)} all-gather(bf16[16,2048]{1,0:T(8,128)(2,1)S(1)} %get-tuple-element.8), channel_id=8, replica_groups=mesh['sp'=16,'tp_0'=4,'tp_1'=2] {'tp_0'}, dimensions={0}, use_global_device_ids=true | all-gather | bytes 327680 | tf_op jit(solution)/shard_map/all_gather | solution.py:39
  239.1 4.5 %all-gather.7 = bf16[8,16,2048]{2,1,0:T(8,128)(2,1)S(1)} all-gather(bf16[4,16,2048]{2,1,0:T(8,128)(2,1)S(1)} %bitcast.233), channel_id=9, replica_groups=mesh['sp'=16,'tp_0'=4,'tp_1'=2] {'tp_1'}, dimensions={0}, use_global_device_ids=true | all-gather | bytes 786432 | tf_op jit(solution)/shard_map/all_gather | solution.py:39
  243.7 1.9 all-gather.4
  245.6 11.3 %all-gather.5 = bf16[8,16,2048]{2,1,0:T(8,128)(2,1)S(1)} all-gather(bf16[2,16,2048]{2,1,0:T(8,128)(2,1)S(1)} %bitcast.238), channel_id=7, replica_groups=mesh['sp'=16,'tp_0'=4,'tp_1'=2] {'tp_0'}, dimensions={0}, use_global_device_ids=true | all-gather | bytes 655360 | tf_op jit(solution)/shard_map/all_gather | solution.py:39
  256.9 0.1 pad_maximum_fusion.1
  257.0 1.3 fusion.82
  258.3 6.0 %all-gather.19.cloned.1.call-done = bf16[8192,512]{1,0:T(8,128)(2,1)} async-done(((bf16[512,512]{1,0:T(8,128)(2,1)}), bf16[8192,512]{1,0:T(8,128)(2,1)}) %all-gather.19.cloned.1.call-update) | async-done | bytes 8388624 | tf_op jit(solution)/shard_map/all_gather | solution.py:117
  264.3 11.6 %bitcast_reduce_fusion = (f32[256,2]{0,1:T(2,128)S(1)}, f32[8192,256,2]{1,0,2:T(8,128)}) fusion(f32[2]{0:T(128)S(1)} %get-tuple-element.15, bf16[32,2,8,512]{3,2,1,0:T(8,128)(2,1)S(1)} %bitcast.245, bf16[8192,512]{1,0:T(8,128)(2,1)} %all-gather.19.cloned.1.call-done), kind=kOutput, calls=%fused_computation.1 | convolution fusion | flops 4303355392 | bytes 25692168 | tf_op jit(solution)/shard_map/tkgd,nkd->tkgn/dot_general | solution.py:123
  275.9 8.8 %fusion.4 = f32[256,2]{0,1:T(2,128)S(1)} fusion(f32[8192,256,2]{1,0,2:T(8,128)} %get-tuple-element.20, f32[256,2]{0,1:T(2,128)S(1)} %broadcast_maximum_fusion, f32[2]{0:T(128)S(1)} %get-tuple-element.15), kind=kLoop, calls=%fused_computation.10 | loop fusion | flops 12582400 | bytes 16781320 | tf_op jit(solution)/shard_map/reduce_sum | solution.py:129
  284.8 52.1 %all-gather.17.cloned.1.call-done = bf16[8192,512]{1,0:T(8,128)(2,1)} async-done(((bf16[512,512]{1,0:T(8,128)(2,1)}), bf16[8192,512]{1,0:T(8,128)(2,1)}) %all-gather.17.cloned.1.call-update) | async-done | bytes 8388624 | tf_op jit(solution)/shard_map/all_gather | solution.py:120
  336.8 12.8 %fusion.90 = bf16[1,512,256,2]{2,1,3,0:T(8,128)(2,1)S(1)} fusion(f32[8192,256,2]{1,0,2:T(8,128)} %get-tuple-element.20, f32[256,2]{0,1:T(2,128)S(1)} %broadcast_maximum_fusion, f32[2]{0:T(128)S(1)} %get-tuple-element.15, bf16[8192,512]{1,0:T(8,128)(2,1)} %all-gather.17.cloned.1.call-done, f32[256,2]{0,1:T(2,128)S(1)} %fusion.4), kind=kOutput, calls=%fused_computation.70 | convolution fusion | flops 4308074496 | bytes 25694216 | tf_op jit(solution)/shard_map/tkgn,nkd->tkgd/dot_general | solution.py:130
  349.6 4.4 %fusion.42 = bf16[256,2048]{1,0:T(8,128)(2,1)} fusion(bf16[256,1024]{0,1:T(8,128)(2,1)S(1)} %bitcast.248, bf16[2,1024,2048]{2,1,0:T(8,128)(2,1)} %param.17), kind=kOutput, calls=%fused_computation.46 | convolution fusion | flops 1074266112 | bytes 5767168 | tf_op jit(solution)/shard_map/dot_general | solution.py:140
  354.1 5.1 %all-to-all-start.2 = ((bf16[8,32,2048]{2,1,0:T(8,128)(2,1)}), bf16[8,32,2048]{2,1,0:T(8,128)(2,1)S(1)}, u32[]{:S(2)}, u32[]{:S(2)}) async-start(bf16[8,32,2048]{2,1,0:T(8,128)(2,1)} %bitcast.45), calls=%async_computation.2 | async-start | bytes 2097152 | tf_op jit(solution)/shard_map/all_to_all | solution.py:66
  359.2 15.0 %all-to-all-done.2 = bf16[8,32,2048]{2,1,0:T(8,128)(2,1)S(1)} async-done(((bf16[8,32,2048]{2,1,0:T(8,128)(2,1)}), bf16[8,32,2048]{2,1,0:T(8,128)(2,1)S(1)}, u32[]{:S(2)}, u32[]{:S(2)}) %all-to-all-start.2) | async-done | bytes 1048608 | tf_op jit(solution)/shard_map/all_to_all | solution.py:66
  374.1 0.1 convert_reduce_fusion
  374.3 0.2 multiply_reduce_fusion
  374.5 0.8 multiply_multiply_fusion
  (39 shorter events, 0.3 us)
Async XLA Ops:
  6.5 8.4 %copy-start.3 = (bf16[2,2048]{1,0:T(2,128)(2,1)S(1)}, bf16[2,2048]{1,0:T(2,128)(2,1)}, u32[]{:S(2)}) copy-start(bf16[2,2048]{1,0:T(2,128)(2,1)} %param.13) | copy-start | bytes 24580
  9.1 32.0 %all-to-all-start = ((bf16[8,64,2048]{2,1,0:T(8,128)(2,1)}), bf16[8,64,2048]{2,1,0:T(8,128)(2,1)S(1)}, u32[]{:S(2)}, u32[]{:S(2)}) async-start(bf16[8,64,2048]{2,1,0:T(8,128)(2,1)} %broadcast_in_dim.2), calls=%async_computation | async-start | bytes 4194304 | tf_op jit(solution)/shard_map/all_to_all | solution.py:22
  14.9 104.0 %all-gather.15.cloned.1.call-start = ((), (), s32[]{:S(2)}) async-start(), calls=%async_computation.4 | async-start | bytes 8912896 | tf_op jit(solution)/shard_map/all_gather | solution.py:117
  41.1 3.9 %copy-start.7 = (bf16[2,2048,512]{2,1,0:T(8,128)(2,1)S(1)}, bf16[2,2048,512]{2,1,0:T(8,128)(2,1)}, u32[]{:S(2)}) copy-start(bf16[2,2048,512]{2,1,0:T(8,128)(2,1)} %param.15) | copy-start | bytes 12582916
  43.7 1.3 copy-start.2
  47.1 4.6 %copy-start.1 = (bf16[8,64,2048]{2,1,0:T(8,128)(2,1)S(1)}, bf16[8,64,2048]{2,1,0:T(8,128)(2,1)}, u32[]{:S(2)}) copy-start(bf16[8,64,2048]{2,1,0:T(8,128)(2,1)} %get-tuple-element.6) | copy-start | bytes 6291460
  47.1 144.4 %all-gather.13.cloned.1.call-start = ((), (), s32[]{:S(2)}) async-start(), calls=%async_computation.3 | async-start | bytes 8912896 | tf_op jit(solution)/shard_map/all_gather | solution.py:120
  51.6 212.6 %all-gather.19.cloned.1.call-start = ((), (), s32[]{:S(2)}) async-start(), calls=%async_computation.6 | async-start | bytes 8912896 | tf_op jit(solution)/shard_map/all_gather | solution.py:117
  55.3 3.8 copy-start
  55.3 3.9 %copy-start.4 = (bf16[2,2048]{1,0:T(2,128)(2,1)S(1)}, bf16[2,2048]{1,0:T(2,128)(2,1)}, u32[]{:S(2)}) copy-start(bf16[2,2048]{1,0:T(2,128)(2,1)} %param.12) | copy-start | bytes 24580
  55.4 31.6 %copy-start.6 = (f32[2,2]{1,0:T(2,128)S(1)}, f32[2,2]{1,0:T(2,128)}, u32[]{:S(2)}) copy-start(f32[2,2]{1,0:T(2,128)} %param.18) | copy-start | bytes 52
  55.4 281.4 %all-gather.17.cloned.1.call-start = ((), (), s32[]{:S(2)}) async-start(), calls=%async_computation.5 | async-start | bytes 8912896 | tf_op jit(solution)/shard_map/all_gather | solution.py:120
  204.4 52.6 %slice-start = ((s8[8388608]{0:T(1024)(128)(4,1)}), s8[4194304]{0:T(1024)(128)(4,1)S(1)}, s32[]{:S(2)}) async-start(s8[8388608]{0:T(1024)(128)(4,1)} %bitcast.243), calls=%async_computation.7 | async-start | bytes 8388608
  208.1 48.9 %slice-start.1 = ((s8[8388608]{0:T(1024)(128)(4,1)}), s8[4194304]{0:T(1024)(128)(4,1)S(1)}, s32[]{:S(2)}) async-start(s8[8388608]{0:T(1024)(128)(4,1)} %bitcast.243), calls=%async_computation.8 | async-start | bytes 8388608
  349.6 9.5 %copy-start.5 = (bf16[2048]{0:T(1024)(128)(2,1)S(1)}, bf16[2048]{0:T(1024)(128)(2,1)}, u32[]{:S(2)}) copy-start(bf16[2048]{0:T(1024)(128)(2,1)} %param.19) | copy-start | bytes 12292
  354.1 20.1 %all-to-all-start.2 = ((bf16[8,32,2048]{2,1,0:T(8,128)(2,1)}), bf16[8,32,2048]{2,1,0:T(8,128)(2,1)S(1)}, u32[]{:S(2)}, u32[]{:S(2)}) async-start(bf16[8,32,2048]{2,1,0:T(8,128)(2,1)} %bitcast.45), calls=%async_computation.2 | async-start | bytes 2097152 | tf_op jit(solution)/shard_map/all_to_all | solution.py:66
Sparse Core Ops, SparseCore 0:
  47.3 71.5 all-gather.14
  121.0 70.5 all-gather.12
  193.7 70.5 all-gather.18
  266.3 70.5 all-gather.16
where the time goes:
time: 382 us
  waiting for transfers between devices  180 us (47%)
  blocking collectives  75.9 us (20%)
  matrix products  75.6 us (20%)
  other arithmetic  22.3 us (6%)
  between operations  13.3 us (3%)
  starting transfers between devices  11 us (3%)
  local copies, waits for them, and re-layouts  4.03 us (1%)
    all_gather x2, waiting for transfers between devices, per_device(): lax.all_gather(value_rows, 'sp', axis=0, tiled=True)  104 us
    all_gather x8, blocking collectives, gather_in_order(): pieces = lax.all_gather(pieces, axes[k])  55.9 us
    all_gather x2, waiting for transfers between devices, per_device(): lax.all_gather(key_rows, 'sp', axis=0, tiled=True)  34.2 us
    all_to_all x1, waiting for transfers between devices, copy_for_each(): return lax.all_to_all(copies, axis, split_axis=0, concat_axis=0, tiled=True)  26.2 us
    dot_general x2, matrix products, per_device(): jnp.einsum('tkgn,nkd->tkgd', exponent.astype(jnp.bfloat16), value_view, p...  25.6 us
    dot_general x2, matrix products, per_device(): jnp.einsum('tkgd,nkd->tkgn', query_view, key_view, preferred_element_type...  23.3 us
    all_to_all x1, blocking collectives, summed_on_arrival(): lax.all_to_all(cut_along(shard, dim, count), axis, 0, 0, tiled=True)  20 us
    reduce_sum x2, other arithmetic, per_device(): row_total = jnp.sum(exponent, axis=-1)  17.7 us
  transfers between devices with their start and end apart: 6, of which 6 were waited for; matrix products, arithmetic and copies ran while one was open for 20% of the time, Pallas kernels for 0%

commit v1 on v0

--- a/solution.py
+++ b/solution.py
@@ -117,9 +117,9 @@
         key_view = lax.all_gather(key_rows, "sp", axis=0, tiled=True).reshape(
             -1, local_shared, HEAD_DIM
         )
-        value_view = lax.all_gather(value_rows, "sp", axis=0, tiled=True).reshape(
-            -1, local_shared, HEAD_DIM
-        )
+        value_view = jnp.concatenate(
+            lax.all_to_all(jnp.stack([value_rows] * lax.axis_size("sp")), "sp", 0, 0), axis=0
+        ).reshape(-1, local_shared, HEAD_DIM)
         scores = jnp.einsum(
             "tkgd,nkd->tkgn", query_view, key_view, preferred_element_type=jnp.float32
         )

time: 382 us -> 509 us (1.33); the launches traced: 382 us -> 500 us
  local copies, waits for them, and re-layouts: 4.03 us -> 63 us
  waiting for transfers between devices: 180 us -> 229 us
  starting transfers between devices: 11 us -> 34.5 us
  blocking collectives: 75.9 us -> 61.7 us
    all_to_all x0 -> x2, waiting for transfers between devices: none -> 188 us  [per_device(): lax.all_to_all(jnp.stack([value_rows] * lax.axis_size('sp')), 'sp', 0, 0)]
    all_gather x2 -> x0, waiting for transfers between devices: 104 us -> none  [per_device(): lax.all_gather(value_rows, 'sp', axis=0, tiled=True)]
    another operation x0 -> x4, local copies, waits for them, and re-layouts: none -> 35.1 us
    all_gather x2, waiting for transfers between devices: 34.2 us -> 0.02 us  [per_device(): lax.all_gather(key_rows, 'sp', axis=0, tiled=True)]
    all_to_all x0 -> x2, local copies, waits for them, and re-layouts: none -> 22.7 us  [per_device(): lax.all_to_all(jnp.stack([value_rows] * lax.axis_size('sp')), 'sp', 0, 0)]
    all_to_all x1 -> x0, blocking collectives: 20 us -> none  [summed_on_arrival(): lax.all_to_all(cut_along(shard, dim, count), axis, 0, 0, tiled=True)]
    all_to_all x0 -> x2, starting transfers between devices: none -> 12.8 us  [per_device(): lax.all_to_all(jnp.stack([value_rows] * lax.axis_size('sp')), 'sp', 0, 0)]
    all_to_all x1 -> x2, starting transfers between devices: 5.09 us -> 15.8 us  [summed_on_arrival(): lax.all_to_all(cut_along(shard, dim, count), axis, 0, 0, tiled=True)]
  transfers between devices with their start and end apart: 6 -> 7, of which waited for: 6 -> 4; matrix products, arithmetic and copies ran while one was open for 20% -> 23% of each run, Pallas kernels for 0% -> 0%
where the time goes in v1:
time: 509 us; the launch traced here: 500 us
  waiting for transfers between devices  229 us (45%)
  matrix products  76.9 us (15%)
  local copies, waits for them, and re-layouts  63 us (12%)
  blocking collectives  61.7 us (12%)
  starting transfers between devices  34.5 us (7%)
  other arithmetic  21.6 us (4%)
  between operations  14 us (3%)
    all_to_all x2, waiting for transfers between devices, per_device(): lax.all_to_all(jnp.stack([value_rows] * lax.axis_size('sp')), 'sp', 0, 0)  188 us
    all_gather x8, blocking collectives, gather_in_order(): pieces = lax.all_gather(pieces, axes[k])  61.7 us
    another operation x2, local copies, waits for them, and re-layouts  27.1 us
    dot_general x2, matrix products, per_device(): jnp.einsum('tkgn,nkd->tkgd', exponent.astype(jnp.bfloat16), value_view, p...  25.7 us
    all_to_all x1, waiting for transfers between devices, copy_for_each(): return lax.all_to_all(copies, axis, split_axis=0, concat_axis=0, tiled=True)  25.4 us
    dot_general x2, matrix products, per_device(): jnp.einsum('tkgd,nkd->tkgn', query_view, key_view, preferred_element_type...  23.2 us
    all_to_all x2, local copies, waits for them, and re-layouts, per_device(): lax.all_to_all(jnp.stack([value_rows] * lax.axis_size('sp')), 'sp', 0, 0)  22.7 us
    reduce_sum x2, other arithmetic, per_device(): row_total = jnp.sum(exponent, axis=-1)  17.1 us
  transfers between devices with their start and end apart: 7, of which 4 were waited for; matrix products, arithmetic and copies ran while one was open for 23% of the time, Pallas kernels for 0%

profile of v1, /device:TPU:1, one launch (start us, length us, event | category | flops | bytes accessed | tf_op | source)
XLA Modules:
  0.0 500.4 jit_solution(1885442664936096526)
XLA Ops:
  6.5 2.5 broadcast_in_dim.2
  9.1 5.8 %all-to-all-start = ((bf16[8,64,2048]{2,1,0:T(8,128)(2,1)}), bf16[8,64,2048]{2,1,0:T(8,128)(2,1)S(1)}, u32[]{:S(2)}, u32[]{:S(2)}) async-start(bf16[8,64,2048]{2,1,0:T(8,128)(2,1)} %broadcast_in_dim.2), calls=%async_computation | async-start | bytes 4194304 | tf_op jit(solution)/shard_map/all_to_all | solution.py:22
  14.9 0.8 fusion.101
  15.7 25.4 %all-to-all-done = bf16[8,64,2048]{2,1,0:T(8,128)(2,1)S(1)} async-done(((bf16[8,64,2048]{2,1,0:T(8,128)(2,1)}), bf16[8,64,2048]{2,1,0:T(8,128)(2,1)S(1)}, u32[]{:S(2)}, u32[]{:S(2)}) %all-to-all-start) | async-done | bytes 2097184 | tf_op jit(solution)/shard_map/all_to_all | solution.py:22
  41.1 0.5 fusion.24
  41.6 2.1 fusion.22
  43.7 1.3 copy-done.2
  45.0 2.1 fusion.70
  47.1 3.5 fusion.67
  50.6 0.2 copy.29
  50.8 4.0 stack.4
  54.8 8.0 %all-to-all-start.1 = ((bf16[16,512,512]{1,2,0:T(8,128)(2,1)}), bf16[16,512,512]{1,2,0:T(8,128)(2,1)}, u32[]{:S(2)}, u32[]{:S(2)}) async-start(bf16[16,512,512]{1,2,0:T(8,128)(2,1)} %stack.4), calls=%async_computation.1 | async-start | bytes 16777216 | tf_op jit(solution)/shard_map/all_to_all | solution.py:121
  62.8 3.7 fusion.76
  66.7 2.8 fusion.73
  69.6 0.2 copy.34
  69.8 140.1 %all-to-all-done.1 = bf16[16,512,512]{1,2,0:T(8,128)(2,1)} async-done(((bf16[16,512,512]{1,2,0:T(8,128)(2,1)}), bf16[16,512,512]{1,2,0:T(8,128)(2,1)}, u32[]{:S(2)}, u32[]{:S(2)}) %all-to-all-start.1) | async-done | bytes 8388640 | tf_op jit(solution)/shard_map/all_to_all | solution.py:121
  209.9 4.0 stack.5
  213.9 4.9 all-to-all-start.3
  218.9 15.3 %all-gather.2 = bf16[64,2048]{1,0:T(8,128)(2,1)S(1)} all-gather(bf16[16,2048]{1,0:T(8,128)(2,1)S(1)} %get-tuple-element.10), channel_id=4, replica_groups=mesh['sp'=16,'tp_0'=4,'tp_1'=2] {'tp_0'}, dimensions={0}, use_global_device_ids=true | all-gather | bytes 327680 | tf_op jit(solution)/shard_map/all_gather | solution.py:39
  234.2 5.0 all-gather.3
  239.2 1.9 all-gather
  241.1 11.6 %all-gather.1 = bf16[8,16,2048]{2,1,0:T(8,128)(2,1)S(1)} all-gather(bf16[2,16,2048]{2,1,0:T(8,128)(2,1)S(1)} %bitcast.224), channel_id=3, replica_groups=mesh['sp'=16,'tp_0'=4,'tp_1'=2] {'tp_0'}, dimensions={0}, use_global_device_ids=true | all-gather | bytes 655360 | tf_op jit(solution)/shard_map/all_gather | solution.py:39
  252.8 3.5 fusion.79
  256.2 11.4 %copy.30 = bf16[16,512,512]{1,0,2:T(8,128)(2,1)} copy(bf16[16,512,512]{1,2,0:T(8,128)(2,1)} %all-to-all-done.1) | data formatting | bytes 16777216 | tf_op jit(solution)/shard_map/all_to_all | solution.py:121
  267.6 13.6 %reshape.224 = bf16[8192,512,1]{0,1,2:T(8,128)(2,1)} reshape(bf16[16,512,512]{1,0,2:T(8,128)(2,1)} %copy.30) | data formatting | bytes 16777216 | tf_op jit(solution)/shard_map/reshape.6
  281.2 11.5 %bitcast_reduce_fusion.1 = (f32[256,2]{0,1:T(2,128)S(1)}, f32[8192,256,2]{1,0,2:T(8,128)}) fusion(f32[2]{0:T(128)S(1)} %get-tuple-element.16, bf16[32,2,8,512]{3,2,1,0:T(8,128)(2,1)S(1)} %bitcast.230, bf16[8192,512]{1,0:T(8,128)(2,1)} %all-gather.11.cloned.1.call-done), kind=kOutput, calls=%fused_computation.5 | convolution fusion | flops 4303355392 | bytes 25692168 | tf_op jit(solution)/shard_map/tkgd,nkd->tkgn/dot_general | solution.py:123
  292.7 8.6 %fusion.2 = f32[256,2]{0,1:T(2,128)S(1)} fusion(f32[8192,256,2]{1,0,2:T(8,128)} %get-tuple-element.18, f32[256,2]{0,1:T(2,128)S(1)} %broadcast_maximum_fusion.1, f32[2]{0:T(128)S(1)} %get-tuple-element.16), kind=kLoop, calls=%fused_computation.8 | loop fusion | flops 12582400 | bytes 16781320 | tf_op jit(solution)/shard_map/reduce_sum | solution.py:129
  301.2 12.9 %fusion.85 = bf16[1,512,256,2]{2,1,3,0:T(8,128)(2,1)S(1)} fusion(bf16[8192,512,1]{0,1,2:T(8,128)(2,1)} %reshape.224, f32[8192,256,2]{1,0,2:T(8,128)} %get-tuple-element.18, f32[256,2]{0,1:T(2,128)S(1)} %broadcast_maximum_fusion.1, f32[2]{0:T(128)S(1)} %get-tuple-element.16, f32[256,2]{0,1:T(2,128)S(1)} %fusion.2), kind=kOutput, calls=%fused_computation.69 | convolution fusion | flops 4308074496 | bytes 25694216 | tf_op jit(solution)/shard_map/tkgn,nkd->tkgd/dot_general | solution.py:130
  314.1 4.5 fusion.37
  318.7 48.2 %all-to-all-done.3 = bf16[16,512,512]{1,2,0:T(8,128)(2,1)} async-done(((bf16[16,512,512]{1,2,0:T(8,128)(2,1)}), bf16[16,512,512]{1,2,0:T(8,128)(2,1)}, u32[]{:S(2)}, u32[]{:S(2)}) %all-to-all-start.3) | async-done | bytes 8388640 | tf_op jit(solution)/shard_map/all_to_all | solution.py:121
  366.8 9.2 %all-to-all-start.2 = ((bf16[8,32,2048]{2,1,0:T(8,128)(2,1)}), bf16[8,32,2048]{2,1,0:T(8,128)(2,1)S(1)}, u32[]{:S(2)}, u32[]{:S(2)}) async-start(bf16[8,32,2048]{2,1,0:T(8,128)(2,1)} %bitcast.21), calls=%async_computation.2 | async-start | bytes 2097152 | tf_op jit(solution)/shard_map/all_to_all | solution.py:66
  376.0 11.3 %copy.35 = bf16[16,512,512]{1,0,2:T(8,128)(2,1)} copy(bf16[16,512,512]{1,2,0:T(8,128)(2,1)} %all-to-all-done.3) | data formatting | bytes 16777216 | tf_op jit(solution)/shard_map/all_to_all | solution.py:121
  387.4 13.5 %reshape.226 = bf16[8192,512,1]{0,1,2:T(8,128)(2,1)} reshape(bf16[16,512,512]{1,0,2:T(8,128)(2,1)} %copy.35) | data formatting | bytes 16777216 | tf_op jit(solution)/shard_map/reshape.31
  400.8 0.1 convert_reduce_fusion.1
  401.0 0.1 multiply_reduce_fusion.1
  401.3 10.4 %all-gather.6 = bf16[64,2048]{1,0:T(8,128)(2,1)S(1)} all-gather(bf16[16,2048]{1,0:T(8,128)(2,1)S(1)} %get-tuple-element.8), channel_id=8, replica_groups=mesh['sp'=16,'tp_0'=4,'tp_1'=2] {'tp_0'}, dimensions={0}, use_global_device_ids=true | all-gather | bytes 327680 | tf_op jit(solution)/shard_map/all_gather | solution.py:39
  411.6 4.5 all-gather.7
  416.2 1.9 all-gather.4
  418.1 11.1 %all-gather.5 = bf16[8,16,2048]{2,1,0:T(8,128)(2,1)S(1)} all-gather(bf16[2,16,2048]{2,1,0:T(8,128)(2,1)S(1)} %bitcast.225), channel_id=7, replica_groups=mesh['sp'=16,'tp_0'=4,'tp_1'=2] {'tp_0'}, dimensions={0}, use_global_device_ids=true | all-gather | bytes 655360 | tf_op jit(solution)/shard_map/all_gather | solution.py:39
  429.3 3.5 fusion.82
  432.8 11.8 %bitcast_reduce_fusion = (f32[256,2]{0,1:T(2,128)S(1)}, f32[8192,256,2]{1,0,2:T(8,128)}) fusion(f32[2]{0:T(128)S(1)} %get-tuple-element.15, bf16[32,2,8,512]{3,2,1,0:T(8,128)(2,1)S(1)} %bitcast.231, bf16[8192,512]{1,0:T(8,128)(2,1)} %all-gather.13.cloned.1.call-done), kind=kOutput, calls=%fused_computation.1 | convolution fusion | flops 4303355392 | bytes 25692168 | tf_op jit(solution)/shard_map/tkgd,nkd->tkgn/dot_general | solution.py:123
  444.6 8.6 %fusion.4 = f32[256,2]{0,1:T(2,128)S(1)} fusion(f32[8192,256,2]{1,0,2:T(8,128)} %get-tuple-element.20, f32[256,2]{0,1:T(2,128)S(1)} %broadcast_maximum_fusion, f32[2]{0:T(128)S(1)} %get-tuple-element.15), kind=kLoop, calls=%fused_computation.10 | loop fusion | flops 12582400 | bytes 16781320 | tf_op jit(solution)/shard_map/reduce_sum | solution.py:129
  453.1 12.8 %fusion.88 = bf16[1,512,256,2]{2,1,3,0:T(8,128)(2,1)S(1)} fusion(bf16[8192,512,1]{0,1,2:T(8,128)(2,1)} %reshape.226, f32[8192,256,2]{1,0,2:T(8,128)} %get-tuple-element.20, f32[256,2]{0,1:T(2,128)S(1)} %broadcast_maximum_fusion, f32[2]{0:T(128)S(1)} %get-tuple-element.15, f32[256,2]{0,1:T(2,128)S(1)} %fusion.4), kind=kOutput, calls=%fused_computation.70 | convolution fusion | flops 4308074496 | bytes 25694216 | tf_op jit(solution)/shard_map/tkgn,nkd->tkgd/dot_general | solution.py:130
  466.0 4.4 fusion.40
  470.4 6.6 %all-to-all-start.4 = ((bf16[8,32,2048]{2,1,0:T(8,128)(2,1)}), bf16[8,32,2048]{2,1,0:T(8,128)(2,1)S(1)}, u32[]{:S(2)}, u32[]{:S(2)}) async-start(bf16[8,32,2048]{2,1,0:T(8,128)(2,1)} %bitcast.43), calls=%async_computation.4 | async-start | bytes 2097152 | tf_op jit(solution)/shard_map/all_to_all | solution.py:66
  477.1 15.0 %all-to-all-done.4 = bf16[8,32,2048]{2,1,0:T(8,128)(2,1)S(1)} async-done(((bf16[8,32,2048]{2,1,0:T(8,128)(2,1)}), bf16[8,32,2048]{2,1,0:T(8,128)(2,1)S(1)}, u32[]{:S(2)}, u32[]{:S(2)}) %all-to-all-start.4) | async-done | bytes 1048608 | tf_op jit(solution)/shard_map/all_to_all | solution.py:66
  492.2 0.2 multiply_reduce_fusion
  492.3 0.8 multiply_multiply_fusion
  (39 shorter events, 0.9 us)
Async XLA Ops:
  9.1 32.0 %all-to-all-start = ((bf16[8,64,2048]{2,1,0:T(8,128)(2,1)}), bf16[8,64,2048]{2,1,0:T(8,128)(2,1)S(1)}, u32[]{:S(2)}, u32[]{:S(2)}) async-start(bf16[8,64,2048]{2,1,0:T(8,128)(2,1)} %broadcast_in_dim.2), calls=%async_computation | async-start | bytes 4194304 | tf_op jit(solution)/shard_map/all_to_all | solution.py:22
  14.9 266.3 %all-gather.11.cloned.1.call-start = ((), (), s32[]{:S(2)}) async-start(), calls=%async_computation.5 | async-start | bytes 8912896 | tf_op jit(solution)/shard_map/all_gather | solution.py:117
  41.1 3.9 copy-start.6
  43.7 1.3 copy-start.2
  54.8 8.0 %copy-start.1 = (bf16[8,64,2048]{2,1,0:T(8,128)(2,1)S(1)}, bf16[8,64,2048]{2,1,0:T(8,128)(2,1)}, u32[]{:S(2)}) copy-start(bf16[8,64,2048]{2,1,0:T(8,128)(2,1)} %get-tuple-element.6) | copy-start | bytes 6291460
  54.8 11.7 %copy-start = (bf16[32,2048]{1,0:T(8,128)(2,1)S(1)}, bf16[32,2048]{1,0:T(8,128)(2,1)}, u32[]{:S(2)}) copy-start(bf16[32,2048]{1,0:T(8,128)(2,1)} %param.10) | copy-start | bytes 393220
  54.8 11.9 %copy-start.3 = (bf16[2,2048]{1,0:T(2,128)(2,1)S(1)}, bf16[2,2048]{1,0:T(2,128)(2,1)}, u32[]{:S(2)}) copy-start(bf16[2,2048]{1,0:T(2,128)(2,1)} %param.12) | copy-start | bytes 24580
  54.8 155.1 %all-to-all-start.1 = ((bf16[16,512,512]{1,2,0:T(8,128)(2,1)}), bf16[16,512,512]{1,2,0:T(8,128)(2,1)}, u32[]{:S(2)}, u32[]{:S(2)}) async-start(bf16[16,512,512]{1,2,0:T(8,128)(2,1)} %stack.4), calls=%async_computation.1 | async-start | bytes 16777216 | tf_op jit(solution)/shard_map/all_to_all | solution.py:121
  62.8 370.0 %all-gather.13.cloned.1.call-start = ((), (), s32[]{:S(2)}) async-start(), calls=%async_computation.6 | async-start | bytes 8912896 | tf_op jit(solution)/shard_map/all_gather | solution.py:117
  213.9 38.8 %copy-start.5 = (f32[2,2]{1,0:T(2,128)S(1)}, f32[2,2]{1,0:T(2,128)}, u32[]{:S(2)}) copy-start(f32[2,2]{1,0:T(2,128)} %param.18) | copy-start | bytes 52
  213.9 152.9 %all-to-all-start.3 = ((bf16[16,512,512]{1,2,0:T(8,128)(2,1)}), bf16[16,512,512]{1,2,0:T(8,128)(2,1)}, u32[]{:S(2)}, u32[]{:S(2)}) async-start(bf16[16,512,512]{1,2,0:T(8,128)(2,1)} %stack.5), calls=%async_computation.3 | async-start | bytes 16777216 | tf_op jit(solution)/shard_map/all_to_all | solution.py:121
  366.8 34.0 %all-to-all-start.2 = ((bf16[8,32,2048]{2,1,0:T(8,128)(2,1)}), bf16[8,32,2048]{2,1,0:T(8,128)(2,1)S(1)}, u32[]{:S(2)}, u32[]{:S(2)}) async-start(bf16[8,32,2048]{2,1,0:T(8,128)(2,1)} %bitcast.21), calls=%async_computation.2 | async-start | bytes 2097152 | tf_op jit(solution)/shard_map/all_to_all | solution.py:66
  466.0 11.1 %copy-start.4 = (bf16[2048]{0:T(1024)(128)(2,1)S(1)}, bf16[2048]{0:T(1024)(128)(2,1)}, u32[]{:S(2)}) copy-start(bf16[2048]{0:T(1024)(128)(2,1)} %param.19) | copy-start | bytes 12292
  470.4 21.6 %all-to-all-start.4 = ((bf16[8,32,2048]{2,1,0:T(8,128)(2,1)}), bf16[8,32,2048]{2,1,0:T(8,128)(2,1)S(1)}, u32[]{:S(2)}, u32[]{:S(2)}) async-start(bf16[8,32,2048]{2,1,0:T(8,128)(2,1)} %bitcast.43), calls=%async_computation.4 | async-start | bytes 2097152 | tf_op jit(solution)/shard_map/all_to_all | solution.py:66
Sparse Core Ops, SparseCore 0:
  47.2 178.4 all-gather.10
  227.8 153.6 all-gather.12
